TPU v7x, 32 devices: a whole 2x2x4 slice. The times are simulated.
32 devices in a mesh: rep: 2 (over x), fs: 8 (over z, y), tp: 2 (over core).
Axes of the slice: x: 2, y: 2, z: 4, core: 2. Of those that a mesh axis runs over, the one named last changes fastest.
Arguments:
- tokens: bfloat16 [16, 64, 2048], P(('rep', 'fs'), None, 'tp'), may hold values from -6 to 6
- lin_weight: bfloat16 [2048, 1024], P('fs', 'tp'), may hold values from -0.125 to 0.125
- glu_weight: bfloat16 [2048, 1024], P('fs', 'tp'), may hold values from -0.125 to 0.125
- conv_taps: float32 [31, 1024], P(None, 'tp'), may hold values from -4 to 4
- conv_gain: float32 [1024], P('tp'), may hold values from 0.1 to 1.9
- conv_out_weight: bfloat16 [1024, 2048], P('tp', 'fs'), may hold values from -0.1875 to 0.1875
- mix_gain: float32 [2048], replicated, may hold values from 0.1 to 1.9
- ff_gate: bfloat16 [2048, 5632], P('fs', 'tp'), may hold values from -0.125 to 0.125
- ff_up: bfloat16 [2048, 5632], P('fs', 'tp'), may hold values from -0.125 to 0.125
- ff_down: bfloat16 [5632, 2048], P('tp', 'fs'), may hold values from -0.078125 to 0.078125
- out_gain: float32 [2048], replicated, may hold values from 0.1 to 1.9
Outputs:
- encoded: bfloat16 [16, 64, 2048], P(('rep', 'fs'), None, 'tp')
All inputs are finite; a program needn't handle non-finite values.
Results may differ from a plain program's by a relative error of at most 0.014.
Values may be sent and summed in bfloat16 or wider, within the bound.
No kernel may reach another device: no remote copies, remote signals or barrier semaphores. Data moves between devices by JAX's collectives and lax.ppermute only.
A program may use at most 128 MiB of HBM per device.

v0:
```python
import jax
import jax.numpy as jnp
from jax import lax
from jax.sharding import PartitionSpec as P

D = 2048
CONV = 1024
TAPS = 31
residual_scale = 2.0**0.25
epsilon = 1e-05


def rounded(value):
    return lax.optimization_barrier(value.astype(jnp.bfloat16)).astype(jnp.float32)


def scaled(values, totals, squares, count):
    average = totals[:, None] / count
    second = squares[:, None] / count
    return (values - average) * lax.rsqrt(second - average * average + epsilon)


def exchange(blocks, axis):
    return lax.all_to_all(blocks, axis, 0, 0)


def after(value, *earlier):
    return lax.optimization_barrier((value, *earlier))[0]


def sum_blocks(blocks):
    return jnp.sum(blocks.astype(jnp.float32), axis=0)


def on_device(
    tokens,
    lin_weight,
    glu_weight,
    conv_taps,
    conv_gain,
    conv_out_weight,
    mix_gain,
    ff_gate,
    ff_up,
    ff_down,
    out_gain,
):
    n_fs = lax.axis_size("fs")
    n_tp = lax.axis_size("tp")
    own_tokens = tokens[0]
    seq, feat_width = own_tokens.shape
    offset = lax.axis_index("tp") * feat_width
    width = feat_width * n_tp
    rows = lin_weight.shape[0]
    chans = lin_weight.shape[1]
    units = ff_gate.shape[1] // n_fs
    all_tokens = lax.all_gather(own_tokens, "tp", axis=1, tiled=True)
    row_tokens = exchange(all_tokens.reshape(seq, n_fs, rows).transpose(1, 0, 2), "fs")
    row_tokens = row_tokens.reshape(n_fs * seq, rows)

    def dealt_columns(weight):
        blocks = weight.reshape(rows, n_fs, units).transpose(1, 0, 2)
        return exchange(blocks, "fs").reshape(n_fs * rows, units)

    gate_own = dealt_columns(after(ff_gate, row_tokens))
    up_own = dealt_columns(after(ff_up, row_tokens))
    terms = jnp.concatenate(
        [
            jnp.dot(row_tokens, lin_weight, preferred_element_type=jnp.float32),
            jnp.dot(row_tokens, glu_weight, preferred_element_type=jnp.float32),
        ],
        axis=1,
    ).astype(jnp.bfloat16)
    both = sum_blocks(exchange(terms.reshape(n_fs, seq, 2 * chans), "fs"))
    down_blocks = after(ff_down, both).reshape(n_fs, units, ff_down.shape[1])
    down_own = exchange(down_blocks, "fs").transpose(1, 0, 2).reshape(units, width)
    glu = (both[:, :chans] * jax.nn.sigmoid(both[:, chans:])).astype(jnp.bfloat16)
    margin = (TAPS - 1) // 2
    conv = lax.conv_general_dilated(
        glu.astype(jnp.float32)[None],
        conv_taps[:, None, :],
        (1,),
        [(margin, margin)],
        dimension_numbers=("NWC", "WIO", "NWC"),
        feature_group_count=glu.shape[1],
        precision=lax.Precision.HIGHEST,
    )[0]
    conv_sums, conv_squares = lax.psum((jnp.sum(conv, axis=1), jnp.sum(conv * conv, axis=1)), "tp")
    activated = jax.nn.silu(scaled(conv, conv_sums, conv_squares, CONV) * conv_gain).astype(
        jnp.bfloat16
    )
    conv_terms = jnp.dot(
        activated,
        lax.all_gather(conv_out_weight, "fs", axis=1, tiled=True),
        preferred_element_type=jnp.float32,
    )
    mixed = rounded(
        lax.psum_scatter(
            conv_terms.astype(jnp.bfloat16), "tp", scatter_dimension=1, tiled=True
        ).astype(jnp.float32)
    )
    before = residual_scale * own_tokens.astype(jnp.float32) + mixed
    mix_sums, mix_squares = lax.psum(
        (jnp.sum(before, axis=1), jnp.sum(before * before, axis=1)), "tp"
    )
    gain_own = lax.dynamic_slice_in_dim(mix_gain, offset, feat_width, 0)
    middle_own = (scaled(before, mix_sums, mix_squares, D) * gain_own).astype(jnp.bfloat16)
    middle_half = lax.all_gather(middle_own, "fs", axis=0, tiled=True)
    middle_all = lax.all_gather(middle_half, "tp", axis=1, tiled=True)
    gate = jnp.dot(middle_all, gate_own, preferred_element_type=jnp.float32)
    upward = jnp.dot(middle_all, up_own, preferred_element_type=jnp.float32)
    hidden = (jax.nn.silu(gate) * upward).astype(jnp.bfloat16)
    down_terms = jnp.dot(hidden, down_own, preferred_element_type=jnp.float32)
    halves = down_terms.astype(jnp.bfloat16).reshape(n_fs * seq, n_tp, feat_width)
    over_tp = sum_blocks(exchange(halves.transpose(1, 0, 2), "tp")).astype(jnp.bfloat16)
    over_fs = sum_blocks(exchange(over_tp.reshape(n_fs, seq, feat_width), "fs"))
    forward = rounded(over_fs)
    final = residual_scale * middle_own.astype(jnp.float32) + forward
    out_sums, out_squares = lax.psum((jnp.sum(final, axis=1), jnp.sum(final * final, axis=1)), "tp")
    gain_slice = lax.dynamic_slice_in_dim(out_gain, offset, feat_width, 0)
    encoded = (scaled(final, out_sums, out_squares, D) * gain_slice).astype(jnp.bfloat16)
    return encoded[None]


def solution(mesh):
    return jax.shard_map(
        on_device,
        mesh=mesh,
        in_specs=(
            P(("rep", "fs"), None, "tp"),
            P("fs", "tp"),
            P("fs", "tp"),
            P(None, "tp"),
            P("tp"),
            P("tp", "fs"),
            P(),
            P("fs", "tp"),
            P("fs", "tp"),
            P("tp", "fs"),
            P(),
        ),
        out_specs=P(("rep", "fs"), None, "tp"),
        check_vma=False,
    )
```

profile of v0, /device:TPU:0, one launch (start us, length us, event | category | flops | bytes accessed | tf_op | source)
XLA Modules:
  0.0 260.5 jit_solution(7943047915175370196)
XLA Ops:
  6.5 2.5 all-gather
  9.0 0.1 copy.45
  9.1 16.2 %all_to_all.35 = bf16[8,64,256]{2,1,0:T(8,128)(2,1)S(1)} all-to-all(bf16[8,64,256]{2,1,0:T(8,128)(2,1)S(1)} %bitcast.77), channel_id=1, replica_groups=mesh['rep'=2,'fs'=8,'tp'=2] {'fs'}, dimensions={0} | all-to-all | bytes 524288 | tf_op jit(solution)/shard_map/all_to_all | solution.py:24
  25.3 0.3 convolution_convert_fusion.2
  25.6 0.3 convolution_convert_fusion.3
  25.9 1.1 pad_maximum_fusion
  27.1 3.6 %all-to-all-start.1 = ((bf16[8,64,1024]{2,1,0:T(8,128)(2,1)}), bf16[8,64,1024]{2,1,0:T(8,128)(2,1)S(1)}, u32[]{:S(2)}, u32[]{:S(2)}) async-start(bf16[8,64,1024]{2,1,0:T(8,128)(2,1)} %pad_maximum_fusion), calls=%async_computation.1 | async-start | bytes 2097152 | tf_op jit(solution)/shard_map/all_to_all | solution.py:24
  30.6 0.0 all-gather.5.cloned.1.call-start
  30.7 0.7 all-gather.5.cloned.1.call-update
  31.4 1.6 copy.34
  32.9 31.7 %all-to-all-done.1 = bf16[8,64,1024]{2,1,0:T(8,128)(2,1)S(1)} async-done(((bf16[8,64,1024]{2,1,0:T(8,128)(2,1)}), bf16[8,64,1024]{2,1,0:T(8,128)(2,1)S(1)}, u32[]{:S(2)}, u32[]{:S(2)}) %all-to-all-start.1) | async-done | bytes 1048608 | tf_op jit(solution)/shard_map/all_to_all | solution.py:24
  64.7 3.6 %all-to-all-start.2 = ((bf16[8,256,352]{1,2,0:T(8,128)(2,1)}), bf16[8,256,352]{1,2,0:T(8,128)(2,1)S(1)}, u32[]{:S(2)}, u32[]{:S(2)}) async-start(bf16[8,256,352]{1,2,0:T(8,128)(2,1)} %bitcast.8), calls=%async_computation.3 | async-start | bytes 2883584 | tf_op jit(solution)/shard_map/all_to_all | solution.py:24
  68.3 2.6 copy.36
  70.8 0.2 convert_reduce_fusion
  71.1 1.3 fusion.30
  72.4 0.1 fusion.18
  72.5 2.5 all-reduce.2
  75.0 42.4 %all-to-all-done.2 = bf16[8,256,352]{1,2,0:T(8,128)(2,1)S(1)} async-done(((bf16[8,256,352]{1,2,0:T(8,128)(2,1)}), bf16[8,256,352]{1,2,0:T(8,128)(2,1)S(1)}, u32[]{:S(2)}, u32[]{:S(2)}) %all-to-all-start.2) | async-done | bytes 1441824 | tf_op jit(solution)/shard_map/all_to_all | solution.py:24
  117.4 3.6 %all-to-all-start.3 = ((bf16[8,256,352]{1,2,0:T(8,128)(2,1)}), bf16[8,256,352]{1,2,0:T(8,128)(2,1)S(1)}, u32[]{:S(2)}, u32[]{:S(2)}) async-start(bf16[8,256,352]{1,2,0:T(8,128)(2,1)} %bitcast.10), calls=%async_computation.4 | async-start | bytes 2883584 | tf_op jit(solution)/shard_map/all_to_all | solution.py:24
  121.0 0.0 reduce-scatter.2.cloned.1.call-start
  121.0 0.0 all-gather.5.cloned.1.call-done
  121.1 2.9 %convolution_convert_fusion.1 = bf16[64,2048]{1,0:T(8,128)(2,1)} fusion(bf16[512,2048]{1,0:T(8,128)(2,1)} %all-gather.5.cloned.1.call-done, f32[1,64,512]{2,0,1:T(1,128)S(1)} %get-tuple-element.28, f32[512]{0:T(512)S(1)} %copy-done.7, f32[64]{0:T(128)S(1)} %get-tuple-element.26, f32[64]{0:T(128)S(1)} %get-tuple-element.25), kind=kOutput, calls=%fused_computation.1 | convolution fusion | flops 134610944 | bytes 2492928 | tf_op jit(solution)/shard_map/dot_general | solution.py:92
  123.9 0.0 reduce-scatter.2.cloned.1.call-update
  123.9 0.0 all-gather.7.cloned.1.call-start
  124.0 9.2 %reduce-scatter.2.cloned.1.call-done = bf16[64,1024]{1,0:T(8,128)(2,1)} async-done(((bf16[64,2048]{1,0:T(8,128)(2,1)}), bf16[64,1024]{1,0:T(8,128)(2,1)}) %reduce-scatter.2.cloned.1.call-update) | async-done | bytes 131088 | tf_op jit(solution)/shard_map/reduce_scatter | solution.py:98
  133.2 1.1 fusion.10
  134.3 2.5 all-reduce.1
  136.7 1.7 multiply_convert_fusion.1
  138.4 0.0 all-gather.7.cloned.1.call-update
  138.4 18.6 %all-to-all-done.3 = bf16[8,256,352]{1,2,0:T(8,128)(2,1)S(1)} async-done(((bf16[8,256,352]{1,2,0:T(8,128)(2,1)}), bf16[8,256,352]{1,2,0:T(8,128)(2,1)S(1)}, u32[]{:S(2)}, u32[]{:S(2)}) %all-to-all-start.3) | async-done | bytes 1441824 | tf_op jit(solution)/shard_map/all_to_all | solution.py:24
  157.0 4.3 %all-to-all-start.4 = ((bf16[8,352,256]{2,1,0:T(8,128)(2,1)}), bf16[8,352,256]{2,1,0:T(8,128)(2,1)}, u32[]{:S(2)}, u32[]{:S(2)}) async-start(bf16[8,352,256]{2,1,0:T(8,128)(2,1)} %bitcast.72), calls=%async_computation.5 | async-start | bytes 2883584 | tf_op jit(solution)/shard_map/all_to_all | solution.py:24
  161.3 0.0 all-gather.9.cloned.1.call-start
  161.3 25.7 %all-gather.7.cloned.1.call-done = bf16[512,1024]{1,0:T(8,128)(2,1)} async-done(((bf16[64,1024]{1,0:T(8,128)(2,1)}), bf16[512,1024]{1,0:T(8,128)(2,1)}) %all-gather.7.cloned.1.call-update) | async-done | bytes 1048592 | tf_op jit(solution)/shard_map/all_gather | solution.py:108
  187.1 1.3 copy.42
  188.4 1.3 copy.43
  189.7 13.6 %all-to-all-done.4 = bf16[8,352,256]{2,1,0:T(8,128)(2,1)} async-done(((bf16[8,352,256]{2,1,0:T(8,128)(2,1)}), bf16[8,352,256]{2,1,0:T(8,128)(2,1)}, u32[]{:S(2)}, u32[]{:S(2)}) %all-to-all-start.4) | async-done | bytes 1441824 | tf_op jit(solution)/shard_map/all_to_all | solution.py:24
  203.3 2.7 %copy.44 = bf16[8,44,8,256]{3,2,0,1:T(8,128)(2,1)} copy(bf16[8,44,8,256]{3,2,1,0:T(8,128)(2,1)} %bitcast.25) | data formatting | bytes 2883584 | tf_op jit(solution)/shard_map/reshape | solution.py:76
  205.9 2.5 fusion.31
  208.5 4.6 %convolution_convert_fusion = bf16[512,2048]{1,0:T(8,128)(2,1)S(1)} fusion(bf16[352,2048]{1,0:T(8,128)(2,1)} %bitcast.75, bf16[512,2048]{1,0:T(8,128)(2,1)} %all-gather.9.cloned.1.call-done, bf16[2048,352]{0,1:T(8,128)(2,1)} %bitcast.73, f32[512,352]{0,1:T(8,128)S(1)} %fusion.31), kind=kOutput, calls=%fused_computation | convolution fusion | flops 1478524928 | bytes 7798784 | tf_op jit(solution)/shard_map/dot_general | solution.py:113
  213.1 0.2 copy.59
  213.3 5.4 %all_to_all.36 = bf16[2,512,1024]{2,1,0:T(8,128)(2,1)S(1)} all-to-all(bf16[2,512,1024]{2,1,0:T(8,128)(2,1)S(1)} %bitcast.68), channel_id=1, replica_groups=mesh['rep'=2,'fs'=8,'tp'=2] {'tp'}, dimensions={0} | all-to-all | bytes 4194304 | tf_op jit(solution)/shard_map/all_to_all | solution.py:24
  218.7 1.7 reduce_sum.92
  220.4 3.7 %all-to-all-start.6 = ((bf16[8,64,1024]{2,1,0:T(8,128)(2,1)}), bf16[8,64,1024]{2,1,0:T(8,128)(2,1)S(1)}, u32[]{:S(2)}, u32[]{:S(2)}) async-start(bf16[8,64,1024]{2,1,0:T(8,128)(2,1)} %bitcast.14), calls=%async_computation.7 | async-start | bytes 2097152 | tf_op jit(solution)/shard_map/all_to_all | solution.py:24
  224.1 26.3 %all-to-all-done.6 = bf16[8,64,1024]{2,1,0:T(8,128)(2,1)S(1)} async-done(((bf16[8,64,1024]{2,1,0:T(8,128)(2,1)}), bf16[8,64,1024]{2,1,0:T(8,128)(2,1)S(1)}, u32[]{:S(2)}, u32[]{:S(2)}) %all-to-all-start.6) | async-done | bytes 1048608 | tf_op jit(solution)/shard_map/all_to_all | solution.py:24
  250.4 0.2 reduce_sum.93
  250.5 0.2 fusion.9
  250.7 2.5 all-reduce
  253.2 0.8 fusion.11
  (28 shorter events, 0.2 us)
Async XLA Ops:
  6.5 18.8 %copy-start = (bf16[256,512]{1,0:T(8,128)(2,1)S(1)}, bf16[256,512]{1,0:T(8,128)(2,1)}, u32[]{:S(2)}) copy-start(bf16[256,512]{1,0:T(8,128)(2,1)} %param.13) | copy-start | bytes 786436
  6.5 19.1 %copy-start.5 = (bf16[256,512]{1,0:T(8,128)(2,1)S(1)}, bf16[256,512]{1,0:T(8,128)(2,1)}, u32[]{:S(2)}) copy-start(bf16[256,512]{1,0:T(8,128)(2,1)} %param.12) | copy-start | bytes 786436
  25.9 5.5 %copy-start.2 = (bf16[256,2816]{1,0:T(8,128)(2,1)S(1)}, bf16[256,2816]{1,0:T(8,128)(2,1)}, u32[]{:S(2)}) copy-start(bf16[256,2816]{1,0:T(8,128)(2,1)} %param.18) | copy-start | bytes 4325380
  27.1 37.6 %all-to-all-start.1 = ((bf16[8,64,1024]{2,1,0:T(8,128)(2,1)}), bf16[8,64,1024]{2,1,0:T(8,128)(2,1)S(1)}, u32[]{:S(2)}, u32[]{:S(2)}) async-start(bf16[8,64,1024]{2,1,0:T(8,128)(2,1)} %pad_maximum_fusion), calls=%async_computation.1 | async-start | bytes 2097152 | tf_op jit(solution)/shard_map/all_to_all | solution.py:24
  30.6 90.4 %all-gather.5.cloned.1.call-start = ((), (), s32[]{:S(2)}) async-start(), calls=%async_computation.8 | async-start | bytes 2359296 | tf_op jit(solution)/shard_map/all_gather | solution.py:94
  64.7 52.7 %all-to-all-start.2 = ((bf16[8,256,352]{1,2,0:T(8,128)(2,1)}), bf16[8,256,352]{1,2,0:T(8,128)(2,1)S(1)}, u32[]{:S(2)}, u32[]{:S(2)}) async-start(bf16[8,256,352]{1,2,0:T(8,128)(2,1)} %bitcast.8), calls=%async_computation.3 | async-start | bytes 2883584 | tf_op jit(solution)/shard_map/all_to_all | solution.py:24
  68.3 2.8 %copy-start.8 = (f32[31,512]{1,0:T(8,128)S(1)}, f32[31,512]{1,0:T(8,128)}, u32[]{:S(2)}) copy-start(f32[31,512]{1,0:T(8,128)} %param.14) | copy-start | bytes 190468
  71.1 50.0 %copy-start.7 = (f32[512]{0:T(512)S(1)}, f32[512]{0:T(512)}, u32[]{:S(2)}) copy-start(f32[512]{0:T(512)} %param.15) | copy-start | bytes 6148
  117.4 39.6 %all-to-all-start.3 = ((bf16[8,256,352]{1,2,0:T(8,128)(2,1)}), bf16[8,256,352]{1,2,0:T(8,128)(2,1)S(1)}, u32[]{:S(2)}, u32[]{:S(2)}) async-start(bf16[8,256,352]{1,2,0:T(8,128)(2,1)} %bitcast.10), calls=%async_computation.4 | async-start | bytes 2883584 | tf_op jit(solution)/shard_map/all_to_all | solution.py:24
  121.0 3.0 %copy-start.6 = (f32[2048]{0:T(1024)S(1)}, f32[2048]{0:T(1024)}, u32[]{:S(2)}) copy-start(f32[2048]{0:T(1024)} %param.17) | copy-start | bytes 24580
  121.0 12.2 %copy-start.4 = (bf16[1,64,1024]{2,1,0:T(8,128)(2,1)S(1)}, bf16[1,64,1024]{2,1,0:T(8,128)(2,1)}, u32[]{:S(2)}) copy-start(bf16[1,64,1024]{2,1,0:T(8,128)(2,1)} %param.11) | copy-start | bytes 393220
  121.0 12.2 %reduce-scatter.2.cloned.1.call-start = ((), (), s32[]{:S(2)}) async-start(), calls=%async_computation.9 | async-start | bytes 393216 | tf_op jit(solution)/shard_map/reduce_scatter | solution.py:98
  123.9 63.2 %all-gather.7.cloned.1.call-start = ((), (), s32[]{:S(2)}) async-start(), calls=%async_computation.10 | async-start | bytes 1179648 | tf_op jit(solution)/shard_map/all_gather | solution.py:108
  157.0 46.3 %all-to-all-start.4 = ((bf16[8,352,256]{2,1,0:T(8,128)(2,1)}), bf16[8,352,256]{2,1,0:T(8,128)(2,1)}, u32[]{:S(2)}, u32[]{:S(2)}) async-start(bf16[8,352,256]{2,1,0:T(8,128)(2,1)} %bitcast.72), calls=%async_computation.5 | async-start | bytes 2883584 | tf_op jit(solution)/shard_map/all_to_all | solution.py:24
  161.3 44.6 %all-gather.9.cloned.1.call-start = ((), (), s32[]{:S(2)}) async-start(), calls=%async_computation.11 | async-start | bytes 3145728 | tf_op jit(solution)/shard_map/all_gather | solution.py:109
  189.7 16.2 %copy-start.3 = (bf16[8,44,8,256]{3,2,0,1:T(8,128)(2,1)S(1)}, bf16[8,44,8,256]{3,2,0,1:T(8,128)(2,1)}, u32[]{:S(2)}) copy-start(bf16[8,44,8,256]{3,2,0,1:T(8,128)(2,1)} %copy.42) | copy-start | bytes 4325380
  220.4 30.1 %copy-start.1 = (bf16[64,1024]{1,0:T(8,128)(2,1)S(1)}, bf16[64,1024]{1,0:T(8,128)(2,1)}, u32[]{:S(2)}) copy-start(bf16[64,1024]{1,0:T(8,128)(2,1)} %multiply_convert_fusion.1) | copy-start | bytes 393220
  220.4 32.8 %dynamic-slice-start = ((f32[2048]{0:T(1024)}, s32[]{:T(128)}), f32[1024]{0:T(1024)S(1)}, s32[]{:S(2)}) async-start(f32[2048]{0:T(1024)} %param.21, s32[]{:T(128)} %select_n.4), calls=%async_computation.12 | async-start | bytes 8704 | tf_op jit(solution)/shard_map/dynamic_slice | solution.py:120
  220.4 30.0 %all-to-all-start.6 = ((bf16[8,64,1024]{2,1,0:T(8,128)(2,1)}), bf16[8,64,1024]{2,1,0:T(8,128)(2,1)S(1)}, u32[]{:S(2)}, u32[]{:S(2)}) async-start(bf16[8,64,1024]{2,1,0:T(8,128)(2,1)} %bitcast.14), calls=%async_computation.7 | async-start | bytes 2097152 | tf_op jit(solution)/shard_map/all_to_all | solution.py:24
Sparse Core Ops, SparseCore 0:
  33.5 80.9 all-gather.4
  124.1 9.0 reduce-scatter.1
  138.5 48.5 all-gather.6
  188.5 14.5 all-gather.8
where the time goes:
time: 261 us; the launch traced here: 260 us
  waiting for transfers between devices  168 us (64%)
  blocking collectives  31.5 us (12%)
  starting transfers between devices  18.9 us (7%)
  between operations  13.4 us (5%)
  matrix products  11.9 us (5%)
  local copies, waits for them, and re-layouts  9.7 us (4%)
  other arithmetic  7.01 us (3%)
    all_to_all x5, waiting for transfers between devices, exchange(): return lax.all_to_all(blocks, axis, 0, 0)  132 us
    all_gather x1, waiting for transfers between devices, on_device(): middle_half = lax.all_gather(middle_own, 'fs', axis=0, tiled=True)  25.7 us
    all_to_all x2, blocking collectives, exchange(): return lax.all_to_all(blocks, axis, 0, 0)  21.6 us
    all_to_all x5, starting transfers between devices, exchange(): return lax.all_to_all(blocks, axis, 0, 0)  18.7 us
    reduce_scatter x1, waiting for transfers between devices, on_device(): lax.psum_scatter(conv_terms.astype(jnp.bfloat16), 'tp', scatter_dimension...  9.16 us
  transfers between devices with their start and end apart: 9, of which 7 were waited for; matrix products, arithmetic and copies ran while one was open for 6% of the time, Pallas kernels for 0%

commit v1 on v0

--- a/solution.py
+++ b/solution.py
@@ -106,7 +106,8 @@
     gain_own = lax.dynamic_slice_in_dim(mix_gain, offset, feat_width, 0)
     middle_own = (scaled(before, mix_sums, mix_squares, D) * gain_own).astype(jnp.bfloat16)
     middle_half = lax.all_gather(middle_own, "fs", axis=0, tiled=True)
-    middle_all = lax.all_gather(middle_half, "tp", axis=1, tiled=True)
+    parts = lax.all_gather(middle_half, "tp", axis=0, tiled=False)
+    middle_all = jnp.concatenate(parts, axis=1)
     gate = jnp.dot(middle_all, gate_own, preferred_element_type=jnp.float32)
     upward = jnp.dot(middle_all, up_own, preferred_element_type=jnp.float32)
     hidden = (jax.nn.silu(gate) * upward).astype(jnp.bfloat16)

time: 261 us -> 266 us (1.019)
  local copies, waits for them, and re-layouts: 9.7 us -> 14.2 us
    all_gather x0 -> x1, local copies, waits for them, and re-layouts: none -> 2.85 us  [on_device(): parts = lax.all_gather(middle_half, 'tp', axis=0, tiled=False)]
where the time goes in v1:
time: 266 us; the launch traced here: 265 us
  waiting for transfers between devices  168 us (63%)
  blocking collectives  31.5 us (12%)
  starting transfers between devices  19 us (7%)
  local copies, waits for them, and re-layouts  14.2 us (5%)
  between operations  13.3 us (5%)
  matrix products  12.3 us (5%)
  other arithmetic  7.02 us (3%)
    all_to_all x5, waiting for transfers between devices, exchange(): return lax.all_to_all(blocks, axis, 0, 0)  132 us
    all_gather x1, waiting for transfers between devices, on_device(): middle_half = lax.all_gather(middle_own, 'fs', axis=0, tiled=True)  26 us
    all_to_all x2, blocking collectives, exchange(): return lax.all_to_all(blocks, axis, 0, 0)  21.6 us
    all_to_all x5, starting transfers between devices, exchange(): return lax.all_to_all(blocks, axis, 0, 0)  18.8 us
    reduce_scatter x1, waiting for transfers between devices, on_device(): lax.psum_scatter(conv_terms.astype(jnp.bfloat16), 'tp', scatter_dimension...  9.16 us
  transfers between devices with their start and end apart: 9, of which 7 were waited for; matrix products, arithmetic and copies ran while one was open for 6% of the time, Pallas kernels for 0%

profile of v1, /device:TPU:0, one launch (start us, length us, event | category | flops | bytes accessed | tf_op | source)
XLA Modules:
  0.0 265.3 jit_solution(6308224283904223196)
XLA Ops:
  6.5 2.5 all-gather
  9.0 0.1 copy.48
  9.1 16.2 %all_to_all.35 = bf16[8,64,256]{2,1,0:T(8,128)(2,1)S(1)} all-to-all(bf16[8,64,256]{2,1,0:T(8,128)(2,1)S(1)} %bitcast.84), channel_id=1, replica_groups=mesh['rep'=2,'fs'=8,'tp'=2] {'fs'}, dimensions={0} | all-to-all | bytes 524288 | tf_op jit(solution)/shard_map/all_to_all | solution.py:24
  25.3 0.3 convolution_convert_fusion.2
  25.6 0.3 convolution_convert_fusion.3
  25.9 1.1 pad_maximum_fusion
  27.1 3.6 %all-to-all-start.1 = ((bf16[8,64,1024]{2,1,0:T(8,128)(2,1)}), bf16[8,64,1024]{2,1,0:T(8,128)(2,1)S(1)}, u32[]{:S(2)}, u32[]{:S(2)}) async-start(bf16[8,64,1024]{2,1,0:T(8,128)(2,1)} %pad_maximum_fusion), calls=%async_computation.1 | async-start | bytes 2097152 | tf_op jit(solution)/shard_map/all_to_all | solution.py:24
  30.7 0.0 all-gather.6.cloned.1.call-start
  30.7 0.7 all-gather.6.cloned.1.call-update
  31.4 1.6 copy.37
  33.0 31.7 %all-to-all-done.1 = bf16[8,64,1024]{2,1,0:T(8,128)(2,1)S(1)} async-done(((bf16[8,64,1024]{2,1,0:T(8,128)(2,1)}), bf16[8,64,1024]{2,1,0:T(8,128)(2,1)S(1)}, u32[]{:S(2)}, u32[]{:S(2)}) %all-to-all-start.1) | async-done | bytes 1048608 | tf_op jit(solution)/shard_map/all_to_all | solution.py:24
  64.7 3.6 %all-to-all-start.2 = ((bf16[8,256,352]{1,2,0:T(8,128)(2,1)}), bf16[8,256,352]{1,2,0:T(8,128)(2,1)S(1)}, u32[]{:S(2)}, u32[]{:S(2)}) async-start(bf16[8,256,352]{1,2,0:T(8,128)(2,1)} %bitcast.11), calls=%async_computation.3 | async-start | bytes 2883584 | tf_op jit(solution)/shard_map/all_to_all | solution.py:24
  68.3 2.6 copy.39
  70.9 0.2 convert_reduce_fusion
  71.1 1.3 fusion.30
  72.4 0.1 fusion.18
  72.5 2.5 all-reduce.2
  75.0 42.4 %all-to-all-done.2 = bf16[8,256,352]{1,2,0:T(8,128)(2,1)S(1)} async-done(((bf16[8,256,352]{1,2,0:T(8,128)(2,1)}), bf16[8,256,352]{1,2,0:T(8,128)(2,1)S(1)}, u32[]{:S(2)}, u32[]{:S(2)}) %all-to-all-start.2) | async-done | bytes 1441824 | tf_op jit(solution)/shard_map/all_to_all | solution.py:24
  117.4 3.6 %all-to-all-start.3 = ((bf16[8,256,352]{1,2,0:T(8,128)(2,1)}), bf16[8,256,352]{1,2,0:T(8,128)(2,1)S(1)}, u32[]{:S(2)}, u32[]{:S(2)}) async-start(bf16[8,256,352]{1,2,0:T(8,128)(2,1)} %bitcast.14), calls=%async_computation.4 | async-start | bytes 2883584 | tf_op jit(solution)/shard_map/all_to_all | solution.py:24
  121.0 0.0 reduce-scatter.2.cloned.1.call-start
  121.0 0.0 all-gather.6.cloned.1.call-done
  121.1 2.8 %convolution_convert_fusion.1 = bf16[64,2048]{1,0:T(8,128)(2,1)} fusion(bf16[512,2048]{1,0:T(8,128)(2,1)} %all-gather.6.cloned.1.call-done, f32[1,64,512]{2,0,1:T(1,128)S(1)} %get-tuple-element.28, f32[512]{0:T(512)S(1)} %copy-done.6, f32[64]{0:T(128)S(1)} %get-tuple-element.26, f32[64]{0:T(128)S(1)} %get-tuple-element.25), kind=kOutput, calls=%fused_computation.1 | convolution fusion | flops 134610944 | bytes 2492928 | tf_op jit(solution)/shard_map/dot_general | solution.py:92
  123.9 0.0 all-gather.8.cloned.1.call-start
  124.0 9.2 %reduce-scatter.2.cloned.1.call-done = bf16[64,1024]{1,0:T(8,128)(2,1)} async-done(((bf16[64,2048]{1,0:T(8,128)(2,1)}), bf16[64,1024]{1,0:T(8,128)(2,1)}) %reduce-scatter.2.cloned.1.call-update) | async-done | bytes 131088 | tf_op jit(solution)/shard_map/reduce_scatter | solution.py:98
  133.2 1.1 fusion.10
  134.2 2.5 all-reduce.1
  136.7 1.7 multiply_convert_fusion.1
  138.4 0.0 all-gather.8.cloned.1.call-update
  138.4 18.6 %all-to-all-done.3 = bf16[8,256,352]{1,2,0:T(8,128)(2,1)S(1)} async-done(((bf16[8,256,352]{1,2,0:T(8,128)(2,1)}), bf16[8,256,352]{1,2,0:T(8,128)(2,1)S(1)}, u32[]{:S(2)}, u32[]{:S(2)}) %all-to-all-start.3) | async-done | bytes 1441824 | tf_op jit(solution)/shard_map/all_to_all | solution.py:24
  157.0 4.3 %all-to-all-start.4 = ((bf16[8,352,256]{2,1,0:T(8,128)(2,1)}), bf16[8,352,256]{2,1,0:T(8,128)(2,1)}, u32[]{:S(2)}, u32[]{:S(2)}) async-start(bf16[8,352,256]{2,1,0:T(8,128)(2,1)} %bitcast.79), calls=%async_computation.5 | async-start | bytes 2883584 | tf_op jit(solution)/shard_map/all_to_all | solution.py:24
  161.3 0.0 all-gather.10.cloned.1.call-start
  161.3 26.0 %all-gather.8.cloned.1.call-done = bf16[512,1024]{1,0:T(8,128)(2,1)} async-done(((bf16[64,1024]{1,0:T(8,128)(2,1)}), bf16[512,1024]{1,0:T(8,128)(2,1)}) %all-gather.8.cloned.1.call-update) | async-done | bytes 1048592 | tf_op jit(solution)/shard_map/all_gather | solution.py:108
  187.3 1.3 copy.45
  188.6 1.3 copy.46
  189.9 13.3 %all-to-all-done.4 = bf16[8,352,256]{2,1,0:T(8,128)(2,1)} async-done(((bf16[8,352,256]{2,1,0:T(8,128)(2,1)}), bf16[8,352,256]{2,1,0:T(8,128)(2,1)}, u32[]{:S(2)}, u32[]{:S(2)}) %all-to-all-start.4) | async-done | bytes 1441824 | tf_op jit(solution)/shard_map/all_to_all | solution.py:24
  203.3 2.6 copy.47
  205.9 2.9 %copy.36 = bf16[2,512,1024]{1,2,0:T(8,128)(2,1)S(1)} copy(bf16[2,512,1024]{2,1,0:T(8,128)(2,1)} %bitcast.75) | data formatting | bytes 4194304 | tf_op jit(solution)/shard_map/all_gather | solution.py:109
  208.8 2.3 fusion.31
  211.0 5.3 %convolution_convert_fusion = bf16[512,2048]{1,0:T(8,128)(2,1)} fusion(bf16[352,2048]{1,0:T(8,128)(2,1)} %bitcast.82, bf16[2048,352]{0,1:T(8,128)(2,1)} %bitcast.81, bf16[512,2048]{0,1:T(8,128)(2,1)S(1)} %bitcast.77, f32[512,352]{0,1:T(8,128)S(1)} %fusion.31), kind=kOutput, calls=%fused_computation | convolution fusion | flops 1478524928 | bytes 7798784 | tf_op jit(solution)/shard_map/dot_general | solution.py:114
  216.3 1.8 copy.62
  218.1 5.4 %all_to_all.36 = bf16[2,512,1024]{2,1,0:T(8,128)(2,1)S(1)} all-to-all(bf16[2,512,1024]{2,1,0:T(8,128)(2,1)S(1)} %bitcast.72), channel_id=1, replica_groups=mesh['rep'=2,'fs'=8,'tp'=2] {'tp'}, dimensions={0} | all-to-all | bytes 4194304 | tf_op jit(solution)/shard_map/all_to_all | solution.py:24
  223.5 1.7 reduce_sum.92
  225.2 3.8 %all-to-all-start.6 = ((bf16[8,64,1024]{2,1,0:T(8,128)(2,1)}), bf16[8,64,1024]{2,1,0:T(8,128)(2,1)S(1)}, u32[]{:S(2)}, u32[]{:S(2)}) async-start(bf16[8,64,1024]{2,1,0:T(8,128)(2,1)} %bitcast.18), calls=%async_computation.7 | async-start | bytes 2097152 | tf_op jit(solution)/shard_map/all_to_all | solution.py:24
  229.1 26.1 %all-to-all-done.6 = bf16[8,64,1024]{2,1,0:T(8,128)(2,1)S(1)} async-done(((bf16[8,64,1024]{2,1,0:T(8,128)(2,1)}), bf16[8,64,1024]{2,1,0:T(8,128)(2,1)S(1)}, u32[]{:S(2)}, u32[]{:S(2)}) %all-to-all-start.6) | async-done | bytes 1048608 | tf_op jit(solution)/shard_map/all_to_all | solution.py:24
  255.2 0.2 reduce_sum.93
  255.4 0.2 fusion.9
  255.5 2.5 all-reduce
  258.0 0.8 fusion.11
  (27 shorter events, 0.2 us)
Async XLA Ops:
  6.5 18.8 %copy-start = (bf16[256,512]{1,0:T(8,128)(2,1)S(1)}, bf16[256,512]{1,0:T(8,128)(2,1)}, u32[]{:S(2)}) copy-start(bf16[256,512]{1,0:T(8,128)(2,1)} %param.13) | copy-start | bytes 786436
  6.5 19.1 %copy-start.4 = (bf16[256,512]{1,0:T(8,128)(2,1)S(1)}, bf16[256,512]{1,0:T(8,128)(2,1)}, u32[]{:S(2)}) copy-start(bf16[256,512]{1,0:T(8,128)(2,1)} %param.12) | copy-start | bytes 786436
  25.9 5.5 %copy-start.2 = (bf16[256,2816]{1,0:T(8,128)(2,1)S(1)}, bf16[256,2816]{1,0:T(8,128)(2,1)}, u32[]{:S(2)}) copy-start(bf16[256,2816]{1,0:T(8,128)(2,1)} %param.18) | copy-start | bytes 4325380
  27.1 37.6 %all-to-all-start.1 = ((bf16[8,64,1024]{2,1,0:T(8,128)(2,1)}), bf16[8,64,1024]{2,1,0:T(8,128)(2,1)S(1)}, u32[]{:S(2)}, u32[]{:S(2)}) async-start(bf16[8,64,1024]{2,1,0:T(8,128)(2,1)} %pad_maximum_fusion), calls=%async_computation.1 | async-start | bytes 2097152 | tf_op jit(solution)/shard_map/all_to_all | solution.py:24
  30.7 90.4 %all-gather.6.cloned.1.call-start = ((), (), s32[]{:S(2)}) async-start(), calls=%async_computation.8 | async-start | bytes 2359296 | tf_op jit(solution)/shard_map/all_gather | solution.py:94
  64.7 52.7 %all-to-all-start.2 = ((bf16[8,256,352]{1,2,0:T(8,128)(2,1)}), bf16[8,256,352]{1,2,0:T(8,128)(2,1)S(1)}, u32[]{:S(2)}, u32[]{:S(2)}) async-start(bf16[8,256,352]{1,2,0:T(8,128)(2,1)} %bitcast.11), calls=%async_computation.3 | async-start | bytes 2883584 | tf_op jit(solution)/shard_map/all_to_all | solution.py:24
  68.3 2.8 %copy-start.7 = (f32[31,512]{1,0:T(8,128)S(1)}, f32[31,512]{1,0:T(8,128)}, u32[]{:S(2)}) copy-start(f32[31,512]{1,0:T(8,128)} %param.14) | copy-start | bytes 190468
  71.1 50.0 %copy-start.6 = (f32[512]{0:T(512)S(1)}, f32[512]{0:T(512)}, u32[]{:S(2)}) copy-start(f32[512]{0:T(512)} %param.15) | copy-start | bytes 6148
  117.4 39.6 %all-to-all-start.3 = ((bf16[8,256,352]{1,2,0:T(8,128)(2,1)}), bf16[8,256,352]{1,2,0:T(8,128)(2,1)S(1)}, u32[]{:S(2)}, u32[]{:S(2)}) async-start(bf16[8,256,352]{1,2,0:T(8,128)(2,1)} %bitcast.14), calls=%async_computation.4 | async-start | bytes 2883584 | tf_op jit(solution)/shard_map/all_to_all | solution.py:24
  121.0 3.0 %copy-start.5 = (f32[2048]{0:T(1024)S(1)}, f32[2048]{0:T(1024)}, u32[]{:S(2)}) copy-start(f32[2048]{0:T(1024)} %param.17) | copy-start | bytes 24580
  121.0 12.2 %copy-start.3 = (bf16[1,64,1024]{2,1,0:T(8,128)(2,1)S(1)}, bf16[1,64,1024]{2,1,0:T(8,128)(2,1)}, u32[]{:S(2)}) copy-start(bf16[1,64,1024]{2,1,0:T(8,128)(2,1)} %param.11) | copy-start | bytes 393220
  121.0 12.2 %reduce-scatter.2.cloned.1.call-start = ((), (), s32[]{:S(2)}) async-start(), calls=%async_computation.9 | async-start | bytes 393216 | tf_op jit(solution)/shard_map/reduce_scatter | solution.py:98
  123.9 63.4 %all-gather.8.cloned.1.call-start = ((), (), s32[]{:S(2)}) async-start(), calls=%async_computation.10 | async-start | bytes 1179648 | tf_op jit(solution)/shard_map/all_gather | solution.py:108
  157.0 46.2 %all-to-all-start.4 = ((bf16[8,352,256]{2,1,0:T(8,128)(2,1)}), bf16[8,352,256]{2,1,0:T(8,128)(2,1)}, u32[]{:S(2)}, u32[]{:S(2)}) async-start(bf16[8,352,256]{2,1,0:T(8,128)(2,1)} %bitcast.79), calls=%async_computation.5 | async-start | bytes 2883584 | tf_op jit(solution)/shard_map/all_to_all | solution.py:24
  161.3 44.6 %all-gather.10.cloned.1.call-start = ((), (), s32[]{:S(2)}) async-start(), calls=%async_computation.11 | async-start | bytes 3145728 | tf_op jit(solution)/shard_map/all_gather | solution.py:109
  225.2 30.1 %copy-start.1 = (bf16[64,1024]{1,0:T(8,128)(2,1)S(1)}, bf16[64,1024]{1,0:T(8,128)(2,1)}, u32[]{:S(2)}) copy-start(bf16[64,1024]{1,0:T(8,128)(2,1)} %multiply_convert_fusion.1) | copy-start | bytes 393220
  225.2 32.8 %dynamic-slice-start = ((f32[2048]{0:T(1024)}, s32[]{:T(128)}), f32[1024]{0:T(1024)S(1)}, s32[]{:S(2)}) async-start(f32[2048]{0:T(1024)} %param.21, s32[]{:T(128)} %select_n.4), calls=%async_computation.12 | async-start | bytes 8704 | tf_op jit(solution)/shard_map/dynamic_slice | solution.py:121
  225.2 30.0 %all-to-all-start.6 = ((bf16[8,64,1024]{2,1,0:T(8,128)(2,1)}), bf16[8,64,1024]{2,1,0:T(8,128)(2,1)S(1)}, u32[]{:S(2)}, u32[]{:S(2)}) async-start(bf16[8,64,1024]{2,1,0:T(8,128)(2,1)} %bitcast.18), calls=%async_computation.7 | async-start | bytes 2097152 | tf_op jit(solution)/shard_map/all_to_all | solution.py:24
Sparse Core Ops, SparseCore 0:
  33.5 80.9 all-gather.5
  124.1 9.0 reduce-scatter.1
  138.5 48.7 all-gather.7
  188.7 14.4 all-gather.9
